TPU v7x, 32 devices: a whole 2x2x4 slice. The times are simulated.
32 devices in a mesh: gr: 2 (over x), fs: 8 (over z, y), tp: 2 (over core).
Axes of the slice: x: 2, y: 2, z: 4, core: 2. Of those that a mesh axis runs over, the one named last changes fastest.
Arguments:
- tokens: bfloat16 [16384, 3072], P(('gr', 'fs')), may hold values from -6 to 6
- norm_gain: float32 [3072], P(('gr', 'fs')), may hold values from 0.1 to 1.9
- gate_weight: float32 [8, 3072, 768], P(None, ('gr', 'fs'), 'tp'), may hold values from -0.109375 to 0.109375
- up_weight: float32 [8, 3072, 768], P(None, ('gr', 'fs'), 'tp'), may hold values from -0.109375 to 0.109375
- down_weight: float32 [8, 3072, 768], P(None, ('gr', 'fs'), 'tp'), may hold values from -0.21875 to 0.21875
- group_pick: int32 [16384], P(('gr', 'fs')), may hold values from 0 to 3, as said below
- expert_pick: int32 [16384, 2], P(('gr', 'fs')), may hold values from 0 to 1, as said below
- route_weight: float32 [16384, 2], P(('gr', 'fs')), may hold values from 0.1 to 1
Outputs:
- combined: bfloat16 [16384, 3072], P(('gr', 'fs'), 'tp')
- gate_served: bfloat16 [8, 3072, 768], P('fs', None, 'tp')
- up_served: bfloat16 [8, 3072, 768], P('fs', None, 'tp')
- down_served: bfloat16 [8, 3072, 768], P('fs', None, 'tp')
Inputs may be any that keep to these rules, and one draw needn't show every extreme that they name: `group_pick`: in each aligned block of 1024 rows every group is picked by the same number of rows. `expert_pick`: the 2 entries of a row differ. In each aligned block of 1024 rows, every expert (group and number together) is named exactly 256 times.
All inputs are finite; a program needn't handle non-finite values.
Results may differ from a plain program's by a relative error of at most 0.0092.
Values may be sent and summed in bfloat16 or wider, within the bound.
A program may use at most 128 MiB of HBM per device.

v0:
```python
import jax
import jax.numpy as jnp
from jax import lax
from jax.experimental import pallas as pl
from jax.experimental.pallas import tpu as pltpu
from jax.sharding import PartitionSpec as P

GROUPS = 4


EPS = 1e-06


def local_spread(
    tokens, norm_gain, gate_weight, up_weight, down_weight, group_pick, expert_pick, route_weight
):
    scaled = norm_gain[None, :, None]
    gate_local = (scaled * gate_weight).astype(jnp.bfloat16)
    up_local = (scaled * up_weight).astype(jnp.bfloat16)
    down_local = down_weight.astype(jnp.bfloat16)
    experts, rows_dev, cols_dev = gate_local.shape
    gate_four = gate_local.reshape(experts, 1, rows_dev, cols_dev)
    up_four = up_local.reshape(experts, 1, rows_dev, cols_dev)
    down_four = down_local.reshape(experts, 1, rows_dev, cols_dev)
    gathered = (
        lax.all_gather(gate_four, "gr", axis=1, tiled=True),
        lax.all_gather(up_four, "gr", axis=1, tiled=True),
        lax.all_gather(down_four, "gr", axis=1, tiled=True),
    )
    relaid = (
        lax.all_to_all(gathered[0], "fs", split_axis=0, concat_axis=2, tiled=True),
        lax.all_to_all(gathered[1], "fs", split_axis=0, concat_axis=2, tiled=True),
        lax.all_to_all(gathered[2], "fs", split_axis=0, concat_axis=2, tiled=True),
    )
    gate_new = relaid[0].reshape(1, -1, cols_dev)
    up_new = relaid[1].reshape(1, -1, cols_dev)
    down_new = relaid[2].reshape(1, -1, cols_dev)
    tok_rows, model_width = tokens.shape
    as_float = tokens.astype(jnp.float32)
    normed = (
        as_float * lax.rsqrt(jnp.mean(as_float * as_float, axis=-1, keepdims=True) + EPS)
    ).astype(jnp.bfloat16)
    per_group = experts // GROUPS
    top_count = expert_pick.shape[1]
    capacity = top_count * tok_rows // experts
    flat_ids = (group_pick[:, None] * per_group + expert_pick).reshape(-1)
    onehot = (flat_ids[:, None] == jnp.arange(experts, dtype=jnp.int32)[None, :]).astype(jnp.int32)
    slot_index = jnp.sum(onehot * (jnp.cumsum(onehot, axis=0) - 1), axis=1)
    target = flat_ids * capacity + slot_index
    source = (
        jnp.zeros((experts * capacity,), jnp.int32)
        .at[target]
        .set(jnp.arange(top_count * tok_rows, dtype=jnp.int32) // top_count)
    )
    outgoing = normed[source].reshape(experts, capacity, model_width)
    share = capacity // lax.axis_size("tp")
    start = lax.axis_index("tp") * share
    my_share = lax.dynamic_slice_in_dim(outgoing, start, share, 1)
    landed = lax.all_to_all(my_share, "fs", split_axis=0, concat_axis=1, tiled=True).reshape(
        experts, share, model_width
    )
    arrived = lax.all_gather(landed, "tp", axis=1, tiled=True).reshape(-1, model_width)
    gate_acts = jnp.dot(arrived, gate_new[0], preferred_element_type=jnp.float32)
    up_acts = jnp.dot(arrived, up_new[0], preferred_element_type=jnp.float32)
    hidden = (jax.nn.silu(gate_acts) * up_acts).astype(jnp.bfloat16)
    partial_value = lax.dot_general(
        hidden, down_new[0], (((1,), (1,)), ((), ())), preferred_element_type=jnp.float32
    ).astype(jnp.bfloat16)
    summed = (
        lax.psum_scatter(partial_value, "tp", scatter_dimension=1, tiled=True)
        .astype(jnp.float32)
        .astype(jnp.bfloat16)
    )
    returned = lax.all_to_all(summed, "fs", split_axis=0, concat_axis=0, tiled=True)
    picked = returned[target].reshape(tok_rows, top_count, -1).astype(jnp.float32)
    combined = jnp.sum(route_weight[:, :, None] * picked, axis=1).astype(jnp.bfloat16)
    return (combined, gate_new, up_new, down_new)


def greet(peers):
    barrier = pltpu.get_barrier_semaphore()
    for peer in peers:
        pl.semaphore_signal(barrier, inc=1, device_id=peer, device_id_type=pl.DeviceIdType.MESH)
    pl.semaphore_wait(barrier, len(peers))


def remote(src, dst, send, recv, peer):
    return pltpu.make_async_remote_copy(
        src_ref=src,
        dst_ref=dst,
        send_sem=send,
        recv_sem=recv,
        device_id=peer,
        device_id_type=pl.DeviceIdType.MESH,
    )


def dispatch(tokens_out, gate_out, up_out, down_out):
    groups, share, width = tokens_out.shape
    n_fs, rows, cols = gate_out.shape
    n_gr, n_tp = lax.axis_size("gr"), lax.axis_size("tp")
    members = n_fs // groups
    n_weights = 3

    def kernel(tok, w0, w1, w2, arrived, s0, s1, s2, sends, local, rz, ry, rt, rw, rg):
        fs, gr, tp = lax.axis_index("fs"), lax.axis_index("gr"), lax.axis_index("tp")
        g, j = fs // members, fs % members
        out_w, in_w = (w0, w1, w2), (s0, s1, s2)
        fs_peers = [{"fs": (fs + s) % n_fs} for s in range(1, n_fs)]
        gr_peers = [{"gr": (gr + s) % n_gr} for s in range(1, n_gr)]
        tp_peers = [{"tp": (tp + s) % n_tp} for s in range(1, n_tp)]
        greet(fs_peers + gr_peers + tp_peers)
        started = []

        def send(src, dst, recv, peer):
            copy = remote(src, dst, sends.at[len(started)], recv, peer)
            copy.start()
            started.append(copy)

        def landed(ref, recv):
            remote(ref, ref, sends.at[0], recv, tp_peers[0]).wait_recv()

        for s in range(1, groups):
            z = (g + s) % groups
            send(tok.at[z], arrived.at[tp, j, g], rz.at[g], {"fs": z * members + j})
        for s in range(1, n_fs):
            d = (fs + s) % n_fs
            for w in range(n_weights):
                send(out_w[w].at[d], in_w[w].at[gr, fs], rw.at[w, fs], {"fs": d})
        locals_ = [pltpu.make_async_copy(tok.at[g], arrived.at[tp, j, g], local.at[n_weights])]
        for w in range(n_weights):
            locals_.append(
                pltpu.make_async_copy(out_w[w].at[fs], in_w[w].at[gr, fs], local.at[w])
            )
        for copy in locals_:
            copy.start()

        for s in range(groups):
            z = (g + groups - s) % groups
            slot = arrived.at[tp, j, z]
            if s:
                landed(slot, rz.at[z])
            source = slot if s else tok.at[g]
            for m in range(1, members):
                send(source, slot, ry.at[j, z], {"fs": g * members + (j + m) % members})
            for peer in tp_peers:
                send(source, slot, rt.at[j, z], peer)
        for s in range(n_fs):
            d = (fs + n_fs - s) % n_fs
            for w in range(n_weights):
                slot = in_w[w].at[gr, d]
                if s:
                    landed(slot, rw.at[w, d])
                for peer in gr_peers:
                    send(slot if s else out_w[w].at[fs], slot, rg.at[w, d], peer)
        for m in range(1, members):
            other = (j + m) % members
            for s in range(groups):
                z = (g + groups - s) % groups
                slot = arrived.at[tp, other, z]
                landed(slot, ry.at[other, z])
                for peer in tp_peers:
                    send(slot, slot, rt.at[other, z], peer)
        for t in range(1, n_tp):
            for m in range(members):
                for z in range(groups):
                    landed(arrived.at[(tp + t) % n_tp, m, z], rt.at[m, z])
        for q in range(1, n_gr):
            for w in range(n_weights):
                for d in range(n_fs):
                    landed(in_w[w].at[(gr + q) % n_gr, d], rg.at[w, d])
        for copy in locals_:
            copy.wait()
        for copy in started:
            copy.wait_send()

    n_sends = (
        groups - 1
        + n_weights * (n_fs - 1)
        + groups * (members - 1 + n_tp - 1)
        + n_weights * n_fs * (n_gr - 1)
        + groups * (members - 1) * (n_tp - 1)
    )
    served = jax.ShapeDtypeStruct((n_gr, n_fs, rows, cols), jnp.bfloat16)
    dma = pltpu.SemaphoreType.DMA
    out = pl.pallas_call(
        kernel,
        out_shape=(
            jax.ShapeDtypeStruct((n_tp, members, groups, share, width), jnp.bfloat16),
            served,
            served,
            served,
        ),
        in_specs=[pl.BlockSpec(memory_space=pltpu.VMEM)] * 4,
        out_specs=[pl.BlockSpec(memory_space=pl.ANY)] * 4,
        scratch_shapes=[
            dma((n_sends,)),
            dma((n_weights + 1,)),
            dma((groups,)),
            dma((members, groups)),
            dma((members, groups)),
            dma((n_weights, n_fs)),
            dma((n_weights, n_fs)),
        ],
        compiler_params=pltpu.CompilerParams(
            collective_id=0, has_side_effects=True, vmem_limit_bytes=60 * 2**20
        ),
        name="dispatch",
    )(tokens_out, gate_out, up_out, down_out)
    return out[0], [x.reshape(1, -1, cols) for x in out[1:]]


def give_back(summed, weights_in):
    n_tp, members, groups, share, width = summed.shape

    def kernel(own, weight, home, others, mixed, send_y, recv_y, send_z, recv_z):
        fs = lax.axis_index("fs")
        g, j = fs // members, fs % members
        mates = [{"fs": g * members + (j + m) % members} for m in range(1, members)]
        greet(mates + [{"fs": (g + s) % groups * members + j} for s in range(1, groups)])
        order = [s % groups for s in range(1, groups + 1)]
        copies = []
        for s in order:
            z = (g + s) % groups
            for t in range(n_tp):
                for m in range(1, members):
                    copy = remote(
                        own.at[t, (j + m) % members, z],
                        others.at[members - m - 1, t, z],
                        send_y.at[m - 1, t, s],
                        recv_y.at[members - m - 1, t, z],
                        mates[m - 1],
                    )
                    copy.start()
                    copies.append(copy)
        for s in order:
            z = (g + s) % groups
            for t in range(n_tp):
                total = weight[j, t, z] * own[t, j, z].astype(jnp.float32)
                for m in range(1, members):
                    slot = others.at[m - 1, t, z]
                    remote(
                        slot, slot, send_y.at[0, 0, 0], recv_y.at[m - 1, t, z], mates[m - 1]
                    ).wait_recv()
                    total += weight[(j + m) % members, t, z] * others[m - 1, t, z].astype(
                        jnp.float32
                    )
                if s:
                    mixed[s - 1, t] = total.astype(jnp.bfloat16)
                    copy = remote(
                        mixed.at[s - 1, t],
                        home.at[t, g],
                        send_z.at[t, s - 1],
                        recv_z.at[t, g],
                        {"fs": z * members + j},
                    )
                    copy.start()
                    copies.append(copy)
                else:
                    home[t, g] = total.astype(jnp.bfloat16)
        for s in range(1, groups):
            z = (g + s) % groups
            for t in range(n_tp):
                slot = home.at[t, z]
                remote(
                    slot, slot, send_z.at[0, 0], recv_z.at[t, z], {"fs": z * members + j}
                ).wait_recv()
        for copy in copies:
            copy.wait_send()

    dma = pltpu.SemaphoreType.DMA
    return pl.pallas_call(
        kernel,
        out_shape=jax.ShapeDtypeStruct((n_tp, groups, share, width), jnp.bfloat16),
        in_specs=[pl.BlockSpec(memory_space=pltpu.VMEM)] * 2,
        out_specs=pl.BlockSpec(memory_space=pltpu.VMEM),
        scratch_shapes=[
            pltpu.VMEM((members - 1, n_tp, groups, share, width), jnp.bfloat16),
            pltpu.VMEM((groups - 1, n_tp, share, width), jnp.bfloat16),
            dma((members - 1, n_tp, groups)),
            dma((members - 1, n_tp, groups)),
            dma((n_tp, groups - 1)),
            dma((n_tp, groups)),
        ],
        compiler_params=pltpu.CompilerParams(
            collective_id=1, has_side_effects=True, vmem_limit_bytes=60 * 2**20
        ),
        name="give_back",
    )(summed, weights_in)


def local_whole_group(
    tokens, norm_gain, gate_weight, up_weight, down_weight, group_pick, expert_pick, route_weight
):
    experts, rows_dev, cols_dev = gate_weight.shape
    tok_rows, model_width = tokens.shape
    per_group = experts // GROUPS
    n_tp = lax.axis_size("tp")
    share = tok_rows // GROUPS // n_tp
    own = share * GROUPS
    columns = [[g * per_group + j for g in range(GROUPS)] for j in range(per_group)]

    scaled = norm_gain[None, :, None]
    to_serve = [
        value.astype(jnp.bfloat16) for value in (scaled * gate_weight, scaled * up_weight, down_weight)
    ]

    onehot = (group_pick[None, :] == jnp.arange(GROUPS, dtype=jnp.int32)[:, None]).astype(
        jnp.bfloat16
    )
    row = lax.broadcasted_iota(jnp.int32, (tok_rows, tok_rows), 0)
    col = lax.broadcasted_iota(jnp.int32, (tok_rows, tok_rows), 1)
    before = jnp.dot(onehot, (row < col).astype(jnp.bfloat16), preferred_element_type=jnp.float32)
    rank = jnp.sum(onehot.astype(jnp.float32) * before, axis=0).astype(jnp.int32)
    place = rank // share * own + group_pick * share + rank % share

    as_float = tokens.astype(jnp.float32)
    normed = (
        as_float * lax.rsqrt(jnp.mean(as_float * as_float, axis=-1, keepdims=True) + EPS)
    ).astype(jnp.bfloat16)
    first = lax.axis_index("tp") * own
    slots = first + lax.broadcasted_iota(jnp.int32, (own, tok_rows), 0)
    select = (slots == place[None, :]).astype(jnp.bfloat16)
    outgoing = jnp.dot(select, normed, preferred_element_type=jnp.float32).astype(jnp.bfloat16)

    member = jnp.arange(per_group, dtype=jnp.int32)
    by_member = jnp.sum(
        jnp.where(expert_pick[:, :, None] == member, route_weight[:, :, None], 0.0), axis=1
    )
    weights_out = jnp.sum(
        jnp.where((row == place[None, :])[None], by_member.T[:, None, :], 0.0), axis=2
    )
    weights_out = weights_out.reshape(per_group, n_tp, GROUPS, share)
    weights_in = lax.all_to_all(
        weights_out, "fs", split_axis=2, concat_axis=2, axis_index_groups=columns, tiled=True
    )

    arrived, (gate_new, up_new, down_new) = dispatch(
        outgoing.reshape(GROUPS, share, model_width), *to_serve
    )
    arrived = arrived.reshape(-1, model_width)
    gate_acts = jnp.dot(arrived, gate_new[0], preferred_element_type=jnp.float32)
    up_acts = jnp.dot(arrived, up_new[0], preferred_element_type=jnp.float32)
    hidden = (jax.nn.silu(gate_acts) * up_acts).astype(jnp.bfloat16)
    partial_value = lax.dot_general(
        hidden, down_new[0], (((1,), (1,)), ((), ())), preferred_element_type=jnp.float32
    ).astype(jnp.bfloat16)
    summed = lax.psum_scatter(partial_value, "tp", scatter_dimension=1, tiled=True)
    width = summed.shape[1]
    returned = give_back(
        summed.reshape(n_tp, per_group, GROUPS, share, width), weights_in[..., None]
    ).reshape(tok_rows, width)
    restore = (col == place[:, None]).astype(jnp.bfloat16)
    combined = jnp.dot(restore, returned, preferred_element_type=jnp.float32).astype(jnp.bfloat16)
    return (combined, gate_new, up_new, down_new)


def local(tokens, norm_gain, gate, up, down, group_pick, expert_pick, route_weight):
    whole_group = gate.shape[0] // GROUPS == expert_pick.shape[1]
    body = local_whole_group if whole_group else local_spread
    return body(tokens, norm_gain, gate, up, down, group_pick, expert_pick, route_weight)


def solution(mesh):
    in_specs = (
        P(("gr", "fs"), None),
        P(("gr", "fs")),
        P(None, ("gr", "fs"), "tp"),
        P(None, ("gr", "fs"), "tp"),
        P(None, ("gr", "fs"), "tp"),
        P(("gr", "fs")),
        P(("gr", "fs"), None),
        P(("gr", "fs"), None),
    )
    out_specs = (
        P(("gr", "fs"), "tp"),
        P("fs", None, "tp"),
        P("fs", None, "tp"),
        P("fs", None, "tp"),
    )
    return jax.shard_map(local, mesh=mesh, in_specs=in_specs, out_specs=out_specs, check_vma=False)
```

profile of v0, /device:TPU:0, one launch (start us, length us, event | category | flops | bytes accessed | tf_op | source)
XLA Modules:
  0.0 373.8 jit_solution(15486868101043230147)
XLA Ops:
  7.2 0.0 reduce-scatter.2.cloned.1.call-start
  7.2 1.1 fusion.15
  8.3 0.7 fusion.23
  9.0 0.0 copy-start
  9.0 4.2 %fusion = f32[1024]{0:T(1024)S(1)} fusion(bf16[1024,3072]{1,0:T(8,128)(2,1)} %param.8), kind=kLoop, calls=%fused_computation.2 | loop fusion | flops 9436160 | bytes 6295552 | tf_op jit(solution)/shard_map/reduce_sum | solution.py:319
  13.3 0.0 copy-done
  13.3 1.2 convert_element_type.47.w2
  14.4 8.1 %fusion.5 = bf16[512,3072]{1,0:T(8,128)(2,1)} fusion(bf16[1024,3072]{1,0:T(8,128)(2,1)} %param.8, f32[1024]{0:T(1024)S(1)} %add_rsqrt_fusion, s32[1024]{0:T(1024)S(1)} %fusion.23, s32[512]{0:T(512)S(1)} %iota_add_fusion), kind=kOutput, calls=%fused_computation.8 | convolution fusion | flops 3232759808 | bytes 9447424 | tf_op jit(solution)/shard_map/dot_general | solution.py:324
  22.5 0.0 copy-done.4
  22.5 0.0 copy-done.5
  22.5 0.0 copy-done.8
  22.5 2.0 multiply_convert_fusion.1
  24.5 169.6 %dispatch.1 = (bf16[2,2,4,128,3072]{4,3,2,1,0:T(8,128)(2,1)}, bf16[2,8,192,384]{3,2,1,0:T(8,128)(2,1)}, bf16[2,8,192,384]{3,2,1,0:T(8,128)(2,1)}, bf16[2,8,192,384]{3,2,1,0:T(8,128)(2,1)}) custom-call(bf16[4,128,3072]{2,1,0:T(8,128)(2,1)} %bitcast.19, bf16[8,192,384]{2,1,0:T(8,128)(2,1)} %get-tuple-element.13.w0, bf16[8,192,384]{2,1,0:T(8,128)(2,1)} %get-tuple-element.12.w1, ...), custom_call_target="tpu_custom_call" | custom-call | tf_op jit(solution)/shard_map/dispatch/pallas_call | solution.py:186
  194.1 0.0 copy-start.1
  194.1 11.6 %fusion.29 = f32[2048,384]{1,0:T(8,128)} fusion(bf16[2048,3072]{1,0:T(8,128)(2,1)} %bitcast.29, bf16[3072,384]{1,0:T(8,128)(2,1)} %bitcast.25), kind=kOutput, calls=%fused_computation.47 | convolution fusion | flops 4831838208 | bytes 18087936 | tf_op jit(solution)/shard_map/dot_general | solution.py:342
  205.7 19.9 %convolution_convert_fusion = bf16[2048,3072]{1,0:T(8,128)(2,1)} fusion(bf16[3072,384]{1,0:T(8,128)(2,1)S(1)} %bitcast.21, f32[2048,384]{1,0:T(8,128)} %fusion.29, bf16[2048,3072]{1,0:T(8,128)(2,1)} %bitcast.30, bf16[3072,384]{1,0:T(8,128)(2,1)} %bitcast.23), kind=kOutput, calls=%fused_computation.4 | convolution fusion | flops 9674686464 | bytes 33030144 | tf_op jit(solution)/shard_map/dot_general | solution.py:345
  225.7 0.0 reduce-scatter.2.cloned.1.call-update
  225.7 0.7 copy-done.6
  226.4 0.0 copy-done.7
  226.4 0.8 iota_compare_fusion
  227.2 1.3 select_reduce_fusion
  228.5 0.6 copy.26
  229.2 27.3 %all-to-all-start = ((f32[2,2,4,128]{3,1,0,2:T(2,128)}), f32[2,2,4,128]{3,1,0,2:T(2,128)S(1)}, u32[]{:S(2)}, u32[]{:S(2)}) async-start(f32[2,2,4,128]{3,1,0,2:T(2,128)} %copy.26), calls=%async_computation.1 | async-start | bytes 16384 | tf_op jit(solution)/shard_map/all_to_all | solution.py:334
  256.5 5.6 %all-to-all-done = f32[2,2,4,128]{3,1,0,2:T(2,128)S(1)} async-done(((f32[2,2,4,128]{3,1,0,2:T(2,128)}), f32[2,2,4,128]{3,1,0,2:T(2,128)S(1)}, u32[]{:S(2)}, u32[]{:S(2)}) %all-to-all-start) | async-done | bytes 8224 | tf_op jit(solution)/shard_map/all_to_all | solution.py:334
  262.0 1.3 copy.28.weight
  263.4 3.6 reduce-scatter.2.cloned.1.call-done
  267.0 87.5 %give_back.1 = bf16[2,4,128,1536]{3,2,1,0:T(8,128)(2,1)} custom-call(bf16[2,2,4,128,1536]{4,3,2,1,0:T(8,128)(2,1)} %bitcast.18, f32[2,2,4,128,1]{4,3,2,1,0:T(8,128)} %copy.28.weight), custom_call_target="tpu_custom_call" | custom-call | tf_op jit(solution)/shard_map/give_back/pallas_call | solution.py:272
  354.6 7.0 %fusion.10 = bf16[1024,1536]{1,0:T(8,128)(2,1)} fusion(bf16[1024,1536]{1,0:T(8,128)(2,1)} %bitcast.20, s32[1024]{0:T(1024)S(1)} %fusion.23), kind=kOutput, calls=%fused_computation.14 | convolution fusion | flops 3223846912 | bytes 6295552 | tf_op jit(solution)/shard_map/dot_general | solution.py:354
  361.6 1.4 copy.34
  363.0 1.1 copy-done.2
  364.1 1.4 copy.35
  365.5 1.4 copy.36
  (13 shorter events, 0.1 us)
Async XLA Ops:
  7.2 259.9 %reduce-scatter.2.cloned.1.call-start = ((), (), s32[]{:S(2)}) async-start(), calls=%async_computation.2 | async-start | bytes 18874368 | tf_op jit(solution)/shard_map/reduce_scatter | solution.py:348
  9.0 4.3 %copy-start = (f32[8,192,384]{2,1,0:T(8,128)S(1)}, f32[8,192,384]{2,1,0:T(8,128)}, u32[]{:S(2)}) copy-start(f32[8,192,384]{2,1,0:T(8,128)} %param.12) | copy-start | bytes 7077892
  14.4 8.1 %copy-start.4 = (f32[8,192,384]{2,1,0:T(8,128)S(1)}, f32[8,192,384]{2,1,0:T(8,128)}, u32[]{:S(2)}) copy-start(f32[8,192,384]{2,1,0:T(8,128)} %param.11) | copy-start | bytes 7077892
  14.4 8.1 %copy-start.5 = (f32[8,192,384]{2,1,0:T(8,128)S(1)}, f32[8,192,384]{2,1,0:T(8,128)}, u32[]{:S(2)}) copy-start(f32[8,192,384]{2,1,0:T(8,128)} %param.10) | copy-start | bytes 7077892
  14.4 8.1 %copy-start.8 = (f32[192]{0:T(256)S(1)}, f32[192]{0:T(256)}, u32[]{:S(2)}) copy-start(f32[192]{0:T(256)} %param.9) | copy-start | bytes 2308
  194.1 11.6 %copy-start.1 = (bf16[2,8,192,384]{3,2,1,0:T(8,128)(2,1)S(1)}, bf16[2,8,192,384]{3,2,1,0:T(8,128)(2,1)}, u32[]{:S(2)}) copy-start(bf16[2,8,192,384]{3,2,1,0:T(8,128)(2,1)} %get-tuple-element.11) | copy-start | bytes 7077892
  225.7 0.7 copy-start.6
  225.7 0.7 copy-start.7
  229.2 32.9 %all-to-all-start = ((f32[2,2,4,128]{3,1,0,2:T(2,128)}), f32[2,2,4,128]{3,1,0,2:T(2,128)S(1)}, u32[]{:S(2)}, u32[]{:S(2)}) async-start(f32[2,2,4,128]{3,1,0,2:T(2,128)} %copy.26), calls=%async_computation.1 | async-start | bytes 16384 | tf_op jit(solution)/shard_map/all_to_all | solution.py:334
  354.6 7.0 %copy-start.3 = (bf16[2,8,192,384]{3,2,1,0:T(8,128)(2,1)S(1)}, bf16[2,8,192,384]{3,2,1,0:T(8,128)(2,1)}, u32[]{:S(2)}) copy-start(bf16[2,8,192,384]{3,2,1,0:T(8,128)(2,1)} %get-tuple-element.9) | copy-start | bytes 7077892
  361.6 2.5 copy-start.2
Sparse Core Ops, SparseCore 0:
  225.8 41.1 reduce-scatter.1
where the time goes:
time: 374 us
  Pallas kernels  257 us (69%)
  matrix products  47.7 us (13%)
  starting transfers between devices  27.3 us (7%)
  between operations  14.1 us (4%)
  other arithmetic  10.2 us (3%)
  waiting for transfers between devices  9.25 us (2%)
  local copies, waits for them, and re-layouts  8.01 us (2%)
    pallas_call x1, Pallas kernels, dispatch(): pl.pallas_call(kernel, out_shape=(jax.ShapeDtypeStruct((n_tp, members, gr...  170 us
    pallas_call x1, Pallas kernels, give_back(): pl.pallas_call(kernel, out_shape=jax.ShapeDtypeStruct((n_tp, groups, shar...  87.5 us
    all_to_all x1, starting transfers between devices, local_whole_group(): lax.all_to_all(weights_out, 'fs', split_axis=2, concat_axis=2, axis_index...  27.3 us
    dot_general x1, matrix products, local_whole_group(): lax.dot_general(hidden, down_new[0], (((1,), (1,)), ((), ())), preferred_...  19.9 us
    dot_general x1, matrix products, local_whole_group(): jnp.dot(arrived, gate_new[0], preferred_element_type=jnp.float32)  11.6 us
    dot_general x1, matrix products, local_whole_group(): jnp.dot(select, normed, preferred_element_type=jnp.float32)  8.08 us
  transfers between devices with their start and end apart: 2, of which 2 were waited for; matrix products, arithmetic and copies ran while one was open for 1% of the time, Pallas kernels for 0%

commit v1 on v0

v1 whole, which is shorter than its diff:
```python
import jax
import jax.numpy as jnp
from jax import lax
from jax.experimental import pallas as pl
from jax.experimental.pallas import tpu as pltpu
from jax.sharding import PartitionSpec as P

GROUPS = 4


EPS = 1e-06


def local_spread(
    tokens, norm_gain, gate_weight, up_weight, down_weight, group_pick, expert_pick, route_weight
):
    scaled = norm_gain[None, :, None]
    gate_local = (scaled * gate_weight).astype(jnp.bfloat16)
    up_local = (scaled * up_weight).astype(jnp.bfloat16)
    down_local = down_weight.astype(jnp.bfloat16)
    experts, rows_dev, cols_dev = gate_local.shape
    gate_four = gate_local.reshape(experts, 1, rows_dev, cols_dev)
    up_four = up_local.reshape(experts, 1, rows_dev, cols_dev)
    down_four = down_local.reshape(experts, 1, rows_dev, cols_dev)
    gathered = (
        lax.all_gather(gate_four, "gr", axis=1, tiled=True),
        lax.all_gather(up_four, "gr", axis=1, tiled=True),
        lax.all_gather(down_four, "gr", axis=1, tiled=True),
    )
    relaid = (
        lax.all_to_all(gathered[0], "fs", split_axis=0, concat_axis=2, tiled=True),
        lax.all_to_all(gathered[1], "fs", split_axis=0, concat_axis=2, tiled=True),
        lax.all_to_all(gathered[2], "fs", split_axis=0, concat_axis=2, tiled=True),
    )
    gate_new = relaid[0].reshape(1, -1, cols_dev)
    up_new = relaid[1].reshape(1, -1, cols_dev)
    down_new = relaid[2].reshape(1, -1, cols_dev)
    tok_rows, model_width = tokens.shape
    as_float = tokens.astype(jnp.float32)
    normed = (
        as_float * lax.rsqrt(jnp.mean(as_float * as_float, axis=-1, keepdims=True) + EPS)
    ).astype(jnp.bfloat16)
    per_group = experts // GROUPS
    top_count = expert_pick.shape[1]
    capacity = top_count * tok_rows // experts
    flat_ids = (group_pick[:, None] * per_group + expert_pick).reshape(-1)
    onehot = (flat_ids[:, None] == jnp.arange(experts, dtype=jnp.int32)[None, :]).astype(jnp.int32)
    slot_index = jnp.sum(onehot * (jnp.cumsum(onehot, axis=0) - 1), axis=1)
    target = flat_ids * capacity + slot_index
    source = (
        jnp.zeros((experts * capacity,), jnp.int32)
        .at[target]
        .set(jnp.arange(top_count * tok_rows, dtype=jnp.int32) // top_count)
    )
    outgoing = normed[source].reshape(experts, capacity, model_width)
    share = capacity // lax.axis_size("tp")
    start = lax.axis_index("tp") * share
    my_share = lax.dynamic_slice_in_dim(outgoing, start, share, 1)
    landed = lax.all_to_all(my_share, "fs", split_axis=0, concat_axis=1, tiled=True).reshape(
        experts, share, model_width
    )
    arrived = lax.all_gather(landed, "tp", axis=1, tiled=True).reshape(-1, model_width)
    gate_acts = jnp.dot(arrived, gate_new[0], preferred_element_type=jnp.float32)
    up_acts = jnp.dot(arrived, up_new[0], preferred_element_type=jnp.float32)
    hidden = (jax.nn.silu(gate_acts) * up_acts).astype(jnp.bfloat16)
    partial_value = lax.dot_general(
        hidden, down_new[0], (((1,), (1,)), ((), ())), preferred_element_type=jnp.float32
    ).astype(jnp.bfloat16)
    summed = (
        lax.psum_scatter(partial_value, "tp", scatter_dimension=1, tiled=True)
        .astype(jnp.float32)
        .astype(jnp.bfloat16)
    )
    returned = lax.all_to_all(summed, "fs", split_axis=0, concat_axis=0, tiled=True)
    picked = returned[target].reshape(tok_rows, top_count, -1).astype(jnp.float32)
    combined = jnp.sum(route_weight[:, :, None] * picked, axis=1).astype(jnp.bfloat16)
    return (combined, gate_new, up_new, down_new)


def greet(peers):
    barrier = pltpu.get_barrier_semaphore()
    for peer in peers:
        pl.semaphore_signal(barrier, inc=1, device_id=peer, device_id_type=pl.DeviceIdType.MESH)
    pl.semaphore_wait(barrier, len(peers))


def remote(src, dst, send, recv, peer):
    return pltpu.make_async_remote_copy(
        src_ref=src,
        dst_ref=dst,
        send_sem=send,
        recv_sem=recv,
        device_id=peer,
        device_id_type=pl.DeviceIdType.MESH,
    )


def nearest_first(n):
    return [sorted(range(n), key=lambda z, g=g: (abs(z - g), z)) for g in range(n)]


def dot_nt(a, b):
    return lax.dot_general(a, b, (((1,), (1,)), ((), ())), preferred_element_type=jnp.float32)


def fused(tokens, gain, gate, up, down, group_pick, expert_pick, route_weight):
    experts, rows, cols = gate.shape
    tok_rows, width = tokens.shape
    n_fs = lax.axis_size("fs")
    n_gr = lax.axis_size("gr")
    n = GROUPS
    members = experts // n
    cap = tok_rows // n
    half = cap // 2
    out_w = width // 2
    n_w = 3
    table = nearest_first(n)
    bf16, f32, i32 = jnp.bfloat16, jnp.float32, jnp.int32
    lanes = 128

    def kernel(
        tok_in, gain_ref, w_gate, w_up, w_down, gp_ref, ep_ref, rw_ref,
        out, s_gate, s_up, s_down,
        W, wf, ow, tok, outgoing, arrived, aw, pin, ownp, home, h, pcol, wout, wcol,
        sends, local, served, rwz, rwx, rwy, rdx, rdy, rtz, raz, rtt, rat, rp, rh,
    ):
        fs, gr, tp = lax.axis_index("fs"), lax.axis_index("gr"), lax.axis_index("tp")
        g, y = fs // members, fs % members
        other_y, other_x, other_t = 1 - y, 1 - gr, 1 - tp
        hit = [1 - ((g - c + n) % n + n - 1) // n for c in range(n)]
        zs = [sum(table[c][s] * hit[c] for c in range(n)) for s in range(n)]
        x_peer, y_peer, t_peer = {"gr": other_x}, {"fs": g * members + other_y}, {"tp": other_t}
        z_peers = [{"fs": zs[s] * members + y} for s in range(n)]
        started = []

        def send(src, dst, recv, peer):
            copy = remote(src, dst, sends.at[len(started)], recv, peer)
            copy.start()
            started.append(copy)

        def landed(ref, recv):
            remote(ref, ref, sends.at[0], recv, t_peer).wait_recv()

        def block(j, x, yy, z):
            at = pl.multiple_of((x * n_fs + z * members + yy) * rows, rows)
            return W.at[j, :, pl.ds(at, rows), :]

        w_in = (w_gate, w_up, w_down)
        loads = [
            [
                pltpu.make_async_copy(
                    w_in[w].at[pl.ds(zs[s] * members, members)], wf.at[w, s], local.at[s, w]
                )
                for w in range(n_w)
            ]
            for s in range(n)
        ]
        order = [1, 0] + list(range(2, n))
        for s in order:
            for copy in loads[s]:
                copy.start()
        tok_load = pltpu.make_async_copy(tok_in, tok, local.at[n, 0])
        tok_load.start()
        greet(z_peers[1:] + [x_peer, y_peer, t_peer])

        eye_r = lax.broadcasted_iota(i32, (rows, rows), 0)
        eye_c = lax.broadcasted_iota(i32, (rows, rows), 1)
        gain_col = jnp.sum(jnp.where(eye_r == eye_c, gain_ref[...], 0.0), axis=1, keepdims=True)

        def cast(s, j, w):
            value = wf[w, s, j]
            return ((gain_col * value) if w < 2 else value).astype(bf16)

        for s in order:
            for copy in loads[s]:
                copy.wait()
            for j in range(members):
                for w in range(n_w):
                    if s:
                        ow[s - 1, j, w] = cast(s, j, w)
                    else:
                        at = pl.multiple_of((gr * n_fs + fs) * rows, rows)
                        W[j, w, pl.ds(at, rows), :] = cast(s, j, w)
                if s:
                    send(ow.at[s - 1, j], block(j, gr, y, g), rwz.at[g, j], z_peers[s])
                else:
                    mine = block(j, gr, y, g)
                    send(mine, mine, rwx.at[g, j], x_peer)
                    send(mine, mine, rwy.at[g, j], y_peer)

        gp = gp_ref[...]
        onehot = jnp.where(
            lax.broadcasted_iota(i32, (16, tok_rows), 0) == gp, 1.0, 0.0
        )
        step = 256
        ranks = []
        for c in range(0, tok_rows, step):
            r_i = lax.broadcasted_iota(i32, (tok_rows, step), 0)
            c_i = lax.broadcasted_iota(i32, (tok_rows, step), 1) + c
            before = jnp.dot(
                onehot.astype(bf16),
                jnp.where(r_i < c_i, 1.0, 0.0).astype(bf16),
                preferred_element_type=f32,
            )
            ranks.append(jnp.sum(onehot[:, c : c + step] * before, axis=0, keepdims=True))
        place = gp.astype(f32) * cap + jnp.concatenate(ranks, axis=1)
        l_r = lax.broadcasted_iota(i32, (lanes, lanes), 0)
        l_c = lax.broadcasted_iota(i32, (lanes, lanes), 1)
        eye = l_r == l_c

        def column(row):
            return jnp.sum(jnp.where(eye, row, 0.0), axis=1, keepdims=True)

        for b in range(0, tok_rows, lanes):
            pcol[b : b + lanes, :] = column(place[:, b : b + lanes]).astype(i32)

        for m in range(members):
            value = jnp.zeros((1, tok_rows), f32)
            for k in range(members):
                value += jnp.where(ep_ref[k : k + 1, :] == m, rw_ref[k : k + 1, :], 0.0)
            for b in range(0, tok_rows, lanes):
                wcol[m, b : b + lanes, :] = column(value[:, b : b + lanes])
        place_i = place.astype(i32)

        tok_load.wait()

        def norm(i, _):
            at = pl.ds(pl.multiple_of(i * 64, 64), 64)
            x = tok[at, :].astype(f32)
            scale = lax.rsqrt(jnp.mean(x * x, axis=-1, keepdims=True) + EPS)
            tok[at, :] = (x * scale).astype(bf16)
            return 0

        lax.fori_loop(0, tok_rows // 64, norm, 0)

        first = pl.multiple_of(tp * half, half)
        for s in range(n):
            slots = lax.broadcasted_iota(i32, (half, tok_rows), 0) + (zs[s] * cap + tp * half)
            select = jnp.where(slots == place_i, 1.0, 0.0).astype(bf16)
            here = pcol[...] == lax.broadcasted_iota(i32, (tok_rows, half), 1) + (
                zs[s] * cap + tp * half
            )
            weights = jnp.zeros((8, half), f32)
            for m in range(members):
                row = jnp.sum(jnp.where(here, wcol[m], 0.0), axis=0, keepdims=True)
                weights = jnp.where(lax.broadcasted_iota(i32, (8, half), 0) == m, row, weights)
            span = 512
            target = arrived.at[g, pl.ds(first, half)] if s == 0 else outgoing.at[s - 1]

            def pick(c, _, target=target, select=select):
                at = pl.ds(pl.multiple_of(c * span, span), span)
                target[:, at] = jnp.dot(select, tok[:, at], preferred_element_type=f32).astype(bf16)
                return 0

            lax.fori_loop(0, width // span, pick, 0)
            if s == 0:
                aw[g, tp] = weights
                send(target, target, rtt.at[g], t_peer)
                send(aw.at[g, tp], aw.at[g, tp], rat.at[g], t_peer)
            else:
                wout[s - 1] = weights
                send(target, arrived.at[g, pl.ds(first, half)], rtz.at[g], z_peers[s])
                send(wout.at[s - 1], aw.at[g, tp], raz.at[g], z_peers[s])

        def relay(s):
            from_x, from_y = block(1, other_x, y, zs[s]), block(0, gr, other_y, zs[s])
            landed(from_x, rwx.at[zs[s], 1])
            send(from_x, from_x, rdy.at[zs[s]], y_peer)
            landed(from_y, rwy.at[zs[s], 0])
            send(from_y, from_y, rdx.at[zs[s]], x_peer)

        for s in range(1, n):
            for j in range(members):
                mine = block(j, gr, y, zs[s])
                landed(mine, rwz.at[zs[s], j])
                send(mine, mine, rwx.at[zs[s], j], x_peer)
                send(mine, mine, rwy.at[zs[s], j], y_peer)
            relay(s - 1)
        relay(n - 1)

        def forward(s):
            slot, small = arrived.at[zs[s], pl.ds(first, half)], aw.at[zs[s], tp]
            landed(slot, rtz.at[zs[s]])
            send(slot, slot, rtt.at[zs[s]], t_peer)
            landed(small, raz.at[zs[s]])
            send(small, small, rat.at[zs[s]], t_peer)

        forward(1)
        for s in range(n):
            landed(block(0, other_x, y, zs[s]), rwx.at[zs[s], 0])
            landed(block(1, gr, other_y, zs[s]), rwy.at[zs[s], 1])
            landed(block(0, other_x, other_y, zs[s]), rdx.at[zs[s]])
            landed(block(1, other_x, other_y, zs[s]), rdy.at[zs[s]])
        out_refs = (s_gate, s_up, s_down)
        stores = [
            pltpu.make_async_copy(W.at[y, w], out_refs[w], served.at[w]) for w in range(n_w)
        ]
        for copy in stores:
            copy.start()

        piece = 512
        second = pl.multiple_of(other_t * half, half)

        def chunk(s):
            z = zs[s]
            if s > 1:
                forward(s)
            landed(arrived.at[z, pl.ds(second, half)], rtt.at[z])
            landed(aw.at[z, other_t], rat.at[z])

            def act(j, _):
                rows_in = arrived[z]
                gate_acts = jnp.dot(rows_in, W[j, 0], preferred_element_type=f32)
                up_acts = jnp.dot(rows_in, W[j, 1], preferred_element_type=f32)
                value = gate_acts / (1.0 + jnp.exp(-gate_acts)) * up_acts
                for t in range(2):
                    scale = column(aw[z, t, pl.ds(j, 1), :])
                    at = slice(t * half, (t + 1) * half)
                    h[j, at, :] = (value[at] * scale).astype(bf16)
                return 0

            lax.fori_loop(0, members, act, 0)

            def down_rows(base, c):
                at = pl.ds(pl.multiple_of(base + c * piece, piece), piece)
                return dot_nt(h[0], W[0, 2, at, :]) + dot_nt(h[1], W[1, 2, at, :])

            give = tok.at[pl.ds(s * cap, cap), pl.ds(0, out_w)]
            back = tok.at[pl.ds(s * cap, cap), pl.ds(out_w, out_w)]

            def theirs(c, _):
                at = pl.ds(pl.multiple_of(c * piece, piece), piece)
                give[:, at] = down_rows(other_t * out_w, c).astype(bf16)
                return 0

            def ours(c, _):
                at = pl.ds(pl.multiple_of(c * piece, piece), piece)
                ownp[:, at] = down_rows(tp * out_w, c).astype(bf16).astype(f32)
                return 0

            lax.fori_loop(0, out_w // piece, theirs, 0)
            send(give, pin.at[s], rp.at[s], t_peer)
            lax.fori_loop(0, out_w // piece, ours, 0)
            landed(pin.at[s], rp.at[s])
            total = (ownp[...] + pin[s].astype(f32)).astype(bf16)
            if s:
                back[...] = total
                send(back, home.at[g], rh.at[g], z_peers[s])
            else:
                home[g] = total

        def restore(s):
            z = zs[s]

            def rows_of(b, _):
                at = pl.ds(pl.multiple_of(b * 256, 256), 256)
                slots = lax.broadcasted_iota(i32, (256, cap), 1) + z * cap
                back = jnp.where(slots == pcol[at, :], 1.0, 0.0).astype(bf16)
                value = jnp.dot(back, home[z], preferred_element_type=f32)
                if s:
                    value += out[at, :].astype(f32)
                out[at, :] = value.astype(bf16)
                return 0

            lax.fori_loop(0, tok_rows // 256, rows_of, 0)

        for s in [1, 2, 0] + list(range(3, n)):
            chunk(s)
        for s in range(n):
            if s:
                landed(home.at[zs[s]], rh.at[zs[s]])
            restore(s)
        for copy in stores:
            copy.wait()
        for copy in started:
            copy.wait_send()

    n_sends = (
        (n - 1) * members + 2 * members
        + 2 * n
        + (n - 1) * 2 * members + 2 * n
        + 2 * (n - 1)
        + n + n - 1
    )
    dma = pltpu.SemaphoreType.DMA
    vmem = pltpu.VMEM
    serve = jax.ShapeDtypeStruct((width, cols), bf16)
    any_space = pl.BlockSpec(memory_space=pl.ANY)
    in_vmem = pl.BlockSpec(memory_space=pltpu.VMEM)
    return pl.pallas_call(
        kernel,
        out_shape=(jax.ShapeDtypeStruct((tok_rows, out_w), bf16), serve, serve, serve),
        in_specs=[any_space, in_vmem, any_space, any_space, any_space] + [in_vmem] * 3,
        out_specs=(in_vmem, any_space, any_space, any_space),
        scratch_shapes=[
            vmem((members, n_w, width, cols), bf16),
            vmem((n_w, n, members, rows, cols), f32),
            vmem((n - 1, members, n_w, rows, cols), bf16),
            vmem((tok_rows, width), bf16),
            vmem((n - 1, half, width), bf16),
            vmem((n, cap, width), bf16),
            vmem((n, 2, 8, lanes), f32),
            vmem((n, cap, out_w), bf16),
            vmem((cap, out_w), f32),
            vmem((n, cap, out_w), bf16),
            vmem((members, cap, cols), bf16),
            vmem((tok_rows, 1), i32),
            vmem((n - 1, 8, lanes), f32),
            vmem((members, tok_rows, 1), f32),
            dma((n_sends,)),
            dma((n + 1, n_w)),
            dma((n_w,)),
            dma((n, members)),
            dma((n, members)),
            dma((n, members)),
            dma((n,)),
            dma((n,)),
            dma((n,)),
            dma((n,)),
            dma((n,)),
            dma((n,)),
            dma((n,)),
            dma((n,)),
        ],
        compiler_params=pltpu.CompilerParams(
            collective_id=0, has_side_effects=True, vmem_limit_bytes=63 * 2**20
        ),
        name="fused",
    )(
        tokens, gain[None, :], gate, up, down,
        group_pick[None, :], expert_pick.T, route_weight.T,
    )


def local_whole_group(*args):
    combined, gate_new, up_new, down_new = fused(*args)
    return (combined, gate_new[None], up_new[None], down_new[None])


def local(tokens, norm_gain, gate, up, down, group_pick, expert_pick, route_weight):
    per_group = gate.shape[0] // GROUPS
    fits = (
        per_group == expert_pick.shape[1] == 2
        and lax.axis_size("gr") == lax.axis_size("tp") == 2
        and lax.axis_size("fs") == gate.shape[0]
        and tokens.shape[0] == 2 * GROUPS * 128
    )
    body = local_whole_group if fits else local_spread
    return body(tokens, norm_gain, gate, up, down, group_pick, expert_pick, route_weight)


def solution(mesh):
    in_specs = (
        P(("gr", "fs"), None),
        P(("gr", "fs")),
        P(None, ("gr", "fs"), "tp"),
        P(None, ("gr", "fs"), "tp"),
        P(None, ("gr", "fs"), "tp"),
        P(("gr", "fs")),
        P(("gr", "fs"), None),
        P(("gr", "fs"), None),
    )
    out_specs = (
        P(("gr", "fs"), "tp"),
        P("fs", None, "tp"),
        P("fs", None, "tp"),
        P("fs", None, "tp"),
    )
    return jax.shard_map(local, mesh=mesh, in_specs=in_specs, out_specs=out_specs, check_vma=False)
```

time: 374 us -> 252 us (0.67)
  matrix products: 47.7 us -> 0 us
  starting transfers between devices: 27.3 us -> 0 us
  Pallas kernels: 257 us -> 241 us
  between operations: 14.1 us -> 0.65 us
  other arithmetic: 10.2 us -> 0 us
  waiting for transfers between devices: 9.25 us -> 0 us
    dot_general x5 -> x0, matrix products: 47.7 us -> none  [the longest x1 19.9 us: local_whole_group(): lax.dot_general(hidden, down_new[0], (((1,), (1,)), ((), ())), preferred_...]
    all_to_all x1 -> x0, starting transfers between devices: 27.3 us -> none  [local_whole_group(): lax.all_to_all(weights_out, 'fs', split_axis=2, concat_axis=2, axis_index...]
    pallas_call x2 -> x1, Pallas kernels: 257 us -> 241 us  [fused(): pl.pallas_call(kernel, out_shape=(jax.ShapeDtypeStruct((tok_rows, out_w),...]
    all_to_all x1 -> x0, waiting for transfers between devices: 5.59 us -> none  [local_whole_group(): lax.all_to_all(weights_out, 'fs', split_axis=2, concat_axis=2, axis_index...]
    reduce_sum x3 -> x0, other arithmetic: 5.56 us -> none  [the longest x1 4.23 us: local_whole_group(): jnp.mean(as_float * as_float, axis=-1, keepdims=True) + EPS]
    unnamed x21 -> x10, local copies, waits for them, and re-layouts: 6.04 us -> 10.3 us
  transfers between devices with their start and end apart: 2 -> 0, of which waited for: 2 -> 0; matrix products, arithmetic and copies ran while one was open for 1% -> 0% of each run, Pallas kernels for 0% -> 0%
where the time goes in v1:
time: 252 us
  Pallas kernels  241 us (96%)
  local copies, waits for them, and re-layouts  10.3 us (4%)
    pallas_call x1, Pallas kernels, fused(): pl.pallas_call(kernel, out_shape=(jax.ShapeDtypeStruct((tok_rows, out_w),...  241 us
    unnamed x10, local copies, waits for them, and re-layouts  10.3 us

profile of v1, /device:TPU:0, one launch (start us, length us, event | category | flops | bytes accessed | tf_op | source)
XLA Modules:
  0.0 251.5 jit_solution(13571359212767366144)
XLA Ops:
  0.6 240.5 %fused.1 = (bf16[1024,1536]{1,0:T(8,128)(2,1)}, bf16[3072,384]{1,0:T(8,128)(2,1)}, bf16[3072,384]{1,0:T(8,128)(2,1)}, bf16[3072,384]{1,0:T(8,128)(2,1)}) custom-call(bf16[1024,3072]{1,0:T(8,128)(2,1)} %tok_in.1, f32[1,192]{1,0:T(1,128)} %bitcast.13, f32[8,192,384]{2,1,0:T(8,128)} %w_gate.1, f32[8,192,384]{2,1,0:T(8,128)} %w_up.1, f32[8,192,384]{2,1,0:T(8,128)} %w_down.1, ...), custom_call_target="tpu_custom_call" | custom-call | tf_op jit(solution)/shard_map/fused/pallas_call | solution.py:390
  241.1 0.0 copy-start.2
  241.2 3.9 %copy.16 = bf16[1024,1536]{1,0:T(8,128)(2,1)} copy(bf16[1024,1536]{1,0:T(8,128)(2,1)} %get-tuple-element.16) | data formatting | bytes 6291456
  245.1 0.0 copy-done.2
  245.1 0.0 copy-start.1
  245.1 1.4 copy.17
  246.5 1.1 copy-done.1
  247.6 0.0 copy-start
  247.6 1.4 copy.18
  249.0 1.1 copy-done
  250.1 1.4 copy.19
Async XLA Ops:
  241.1 3.9 %copy-start.2 = (bf16[3072,384]{1,0:T(8,128)(2,1)S(1)}, bf16[3072,384]{1,0:T(8,128)(2,1)}, u32[]{:S(2)}) copy-start(bf16[3072,384]{1,0:T(8,128)(2,1)} %get-tuple-element.9) | copy-start | bytes 7077892
  245.1 2.5 %copy-start.1 = (bf16[3072,384]{1,0:T(8,128)(2,1)S(1)}, bf16[3072,384]{1,0:T(8,128)(2,1)}, u32[]{:S(2)}) copy-start(bf16[3072,384]{1,0:T(8,128)(2,1)} %get-tuple-element.10) | copy-start | bytes 7077892
  247.6 2.5 %copy-start = (bf16[3072,384]{1,0:T(8,128)(2,1)S(1)}, bf16[3072,384]{1,0:T(8,128)(2,1)}, u32[]{:S(2)}) copy-start(bf16[3072,384]{1,0:T(8,128)(2,1)} %get-tuple-element.11) | copy-start | bytes 7077892

commit v2 on v1

--- a/solution.py
+++ b/solution.py
@@ -120,9 +120,9 @@
 
     def kernel(
         tok_in, gain_ref, w_gate, w_up, w_down, gp_ref, ep_ref, rw_ref,
-        out, s_gate, s_up, s_down,
-        W, wf, ow, tok, outgoing, arrived, aw, pin, ownp, home, h, pcol, wout, wcol,
-        sends, local, served, rwz, rwx, rwy, rdx, rdy, rtz, raz, rtt, rat, rp, rh,
+        out, W_own,
+        W_other, wf, ow, tok, outgoing, arrived, aw, pin, ownp, home, h, pcol, wout, wcol,
+        sends, local, rwz, rwx, rwy, rdx, rdy, rtz, raz, rtt, rat, rp, rh,
     ):
         fs, gr, tp = lax.axis_index("fs"), lax.axis_index("gr"), lax.axis_index("tp")
         g, y = fs // members, fs % members
@@ -141,9 +141,11 @@
         def landed(ref, recv):
             remote(ref, ref, sends.at[0], recv, t_peer).wait_recv()
 
+        W = (W_own, W_other)
+
         def block(j, x, yy, z):
             at = pl.multiple_of((x * n_fs + z * members + yy) * rows, rows)
-            return W.at[j, :, pl.ds(at, rows), :]
+            return W[j].at[:, pl.ds(at, rows), :]
 
         w_in = (w_gate, w_up, w_down)
         loads = [
@@ -168,7 +170,7 @@
         gain_col = jnp.sum(jnp.where(eye_r == eye_c, gain_ref[...], 0.0), axis=1, keepdims=True)
 
         def cast(s, j, w):
-            value = wf[w, s, j]
+            value = wf[w, s, (y + j) % members]
             return ((gain_col * value) if w < 2 else value).astype(bf16)
 
         for s in order:
@@ -180,13 +182,13 @@
                         ow[s - 1, j, w] = cast(s, j, w)
                     else:
                         at = pl.multiple_of((gr * n_fs + fs) * rows, rows)
-                        W[j, w, pl.ds(at, rows), :] = cast(s, j, w)
+                        W[j][w, pl.ds(at, rows), :] = cast(s, j, w)
                 if s:
                     send(ow.at[s - 1, j], block(j, gr, y, g), rwz.at[g, j], z_peers[s])
                 else:
                     mine = block(j, gr, y, g)
                     send(mine, mine, rwx.at[g, j], x_peer)
-                    send(mine, mine, rwy.at[g, j], y_peer)
+                    send(mine, block(1 - j, gr, y, g), rwy.at[g, 1 - j], y_peer)
 
         gp = gp_ref[...]
         onehot = jnp.where(
@@ -234,6 +236,7 @@
         lax.fori_loop(0, tok_rows // 64, norm, 0)
 
         first = pl.multiple_of(tp * half, half)
+        held = []
         for s in range(n):
             slots = lax.broadcasted_iota(i32, (half, tok_rows), 0) + (zs[s] * cap + tp * half)
             select = jnp.where(slots == place_i, 1.0, 0.0).astype(bf16)
@@ -259,14 +262,14 @@
                 send(aw.at[g, tp], aw.at[g, tp], rat.at[g], t_peer)
             else:
                 wout[s - 1] = weights
-                send(target, arrived.at[g, pl.ds(first, half)], rtz.at[g], z_peers[s])
-                send(wout.at[s - 1], aw.at[g, tp], raz.at[g], z_peers[s])
+                held.append((wout.at[s - 1], aw.at[g, tp], raz.at[g], z_peers[s]))
+                held.append((target, arrived.at[g, pl.ds(first, half)], rtz.at[g], z_peers[s]))
 
         def relay(s):
-            from_x, from_y = block(1, other_x, y, zs[s]), block(0, gr, other_y, zs[s])
+            from_x, from_y = block(1, other_x, y, zs[s]), block(1, gr, other_y, zs[s])
             landed(from_x, rwx.at[zs[s], 1])
-            send(from_x, from_x, rdy.at[zs[s]], y_peer)
-            landed(from_y, rwy.at[zs[s], 0])
+            send(from_x, block(0, other_x, y, zs[s]), rdy.at[zs[s]], y_peer)
+            landed(from_y, rwy.at[zs[s], 1])
             send(from_y, from_y, rdx.at[zs[s]], x_peer)
 
         for s in range(1, n):
@@ -274,7 +277,10 @@
                 mine = block(j, gr, y, zs[s])
                 landed(mine, rwz.at[zs[s], j])
                 send(mine, mine, rwx.at[zs[s], j], x_peer)
-                send(mine, mine, rwy.at[zs[s], j], y_peer)
+                send(mine, block(1 - j, gr, y, zs[s]), rwy.at[zs[s], 1 - j], y_peer)
+            if s == n - 1:
+                for copy in held:
+                    send(*copy)
             relay(s - 1)
         relay(n - 1)
 
@@ -288,16 +294,9 @@
         forward(1)
         for s in range(n):
             landed(block(0, other_x, y, zs[s]), rwx.at[zs[s], 0])
-            landed(block(1, gr, other_y, zs[s]), rwy.at[zs[s], 1])
-            landed(block(0, other_x, other_y, zs[s]), rdx.at[zs[s]])
-            landed(block(1, other_x, other_y, zs[s]), rdy.at[zs[s]])
-        out_refs = (s_gate, s_up, s_down)
-        stores = [
-            pltpu.make_async_copy(W.at[y, w], out_refs[w], served.at[w]) for w in range(n_w)
-        ]
-        for copy in stores:
-            copy.start()
-
+            landed(block(0, gr, other_y, zs[s]), rwy.at[zs[s], 0])
+            landed(block(1, other_x, other_y, zs[s]), rdx.at[zs[s]])
+            landed(block(0, other_x, other_y, zs[s]), rdy.at[zs[s]])
         piece = 512
         second = pl.multiple_of(other_t * half, half)
 
@@ -308,22 +307,20 @@
             landed(arrived.at[z, pl.ds(second, half)], rtt.at[z])
             landed(aw.at[z, other_t], rat.at[z])
 
-            def act(j, _):
+            for j in range(members):
+                member = (y + j) % members
                 rows_in = arrived[z]
-                gate_acts = jnp.dot(rows_in, W[j, 0], preferred_element_type=f32)
-                up_acts = jnp.dot(rows_in, W[j, 1], preferred_element_type=f32)
+                gate_acts = jnp.dot(rows_in, W[j][0], preferred_element_type=f32)
+                up_acts = jnp.dot(rows_in, W[j][1], preferred_element_type=f32)
                 value = gate_acts / (1.0 + jnp.exp(-gate_acts)) * up_acts
                 for t in range(2):
-                    scale = column(aw[z, t, pl.ds(j, 1), :])
+                    scale = column(aw[z, t, pl.ds(member, 1), :])
                     at = slice(t * half, (t + 1) * half)
                     h[j, at, :] = (value[at] * scale).astype(bf16)
-                return 0
-
-            lax.fori_loop(0, members, act, 0)
 
             def down_rows(base, c):
                 at = pl.ds(pl.multiple_of(base + c * piece, piece), piece)
-                return dot_nt(h[0], W[0, 2, at, :]) + dot_nt(h[1], W[1, 2, at, :])
+                return dot_nt(h[0], W_own[2, at, :]) + dot_nt(h[1], W_other[2, at, :])
 
             give = tok.at[pl.ds(s * cap, cap), pl.ds(0, out_w)]
             back = tok.at[pl.ds(s * cap, cap), pl.ds(out_w, out_w)]
@@ -370,8 +367,6 @@
             if s:
                 landed(home.at[zs[s]], rh.at[zs[s]])
             restore(s)
-        for copy in stores:
-            copy.wait()
         for copy in started:
             copy.wait_send()
 
@@ -384,16 +379,15 @@
     )
     dma = pltpu.SemaphoreType.DMA
     vmem = pltpu.VMEM
-    serve = jax.ShapeDtypeStruct((width, cols), bf16)
     any_space = pl.BlockSpec(memory_space=pl.ANY)
     in_vmem = pl.BlockSpec(memory_space=pltpu.VMEM)
     return pl.pallas_call(
         kernel,
-        out_shape=(jax.ShapeDtypeStruct((tok_rows, out_w), bf16), serve, serve, serve),
+        out_shape=(vmem((tok_rows, out_w), bf16), vmem((n_w, width, cols), bf16)),
         in_specs=[any_space, in_vmem, any_space, any_space, any_space] + [in_vmem] * 3,
-        out_specs=(in_vmem, any_space, any_space, any_space),
+        out_specs=(in_vmem, in_vmem),
         scratch_shapes=[
-            vmem((members, n_w, width, cols), bf16),
+            vmem((n_w, width, cols), bf16),
             vmem((n_w, n, members, rows, cols), f32),
             vmem((n - 1, members, n_w, rows, cols), bf16),
             vmem((tok_rows, width), bf16),
@@ -409,7 +403,6 @@
             vmem((members, tok_rows, 1), f32),
             dma((n_sends,)),
             dma((n + 1, n_w)),
-            dma((n_w,)),
             dma((n, members)),
             dma((n, members)),
             dma((n, members)),
@@ -423,7 +416,7 @@
             dma((n,)),
         ],
         compiler_params=pltpu.CompilerParams(
-            collective_id=0, has_side_effects=True, vmem_limit_bytes=63 * 2**20
+            collective_id=0, has_side_effects=True, vmem_limit_bytes=51 * 2**20
         ),
         name="fused",
     )(
@@ -432,8 +425,42 @@
     )
 
 
+def deliver(combined, served):
+    parts = 4
+    n_w, width, cols = served.shape
+
+    def kernel(src, weights, out, gate, up, down, sems):
+        copies = []
+        for w, dst in enumerate((gate, up, down)):
+            step = width // parts
+            for p in range(parts):
+                at = pl.ds(p * step, step)
+                copies.append(
+                    pltpu.make_async_copy(weights.at[w, at], dst.at[at], sems.at[len(copies)])
+                )
+        step = src.shape[0] // parts
+        for p in range(parts):
+            at = pl.ds(p * step, step)
+            copies.append(pltpu.make_async_copy(src.at[at], out.at[at], sems.at[len(copies)]))
+        for copy in copies:
+            copy.start()
+        for copy in copies:
+            copy.wait()
+
+    serve = jax.ShapeDtypeStruct((width, cols), served.dtype)
+    return pl.pallas_call(
+        kernel,
+        out_shape=(jax.ShapeDtypeStruct(combined.shape, combined.dtype), serve, serve, serve),
+        in_specs=[pl.BlockSpec(memory_space=pltpu.VMEM)] * 2,
+        out_specs=[pl.BlockSpec(memory_space=pl.ANY)] * 4,
+        scratch_shapes=[pltpu.SemaphoreType.DMA(((n_w + 1) * parts,))],
+        compiler_params=pltpu.CompilerParams(vmem_limit_bytes=12 * 2**20),
+        name="deliver",
+    )(combined, served)
+
+
 def local_whole_group(*args):
-    combined, gate_new, up_new, down_new = fused(*args)
+    combined, gate_new, up_new, down_new = deliver(*fused(*args))
     return (combined, gate_new[None], up_new[None], down_new[None])
 
 

time: 252 us -> 228 us (0.905)
  Pallas kernels: 241 us -> 227 us
  local copies, waits for them, and re-layouts: 10.3 us -> 0 us
    pallas_call x1 -> x2, Pallas kernels: 241 us -> 227 us  [the longest x1 223 us: fused(): pl.pallas_call(kernel, out_shape=(vmem((tok_rows, out_w), bf16), vmem((n_...]
    unnamed x10 -> x0, local copies, waits for them, and re-layouts: 10.3 us -> none
where the time goes in v2:
time: 228 us; the launch traced here: 227 us
  Pallas kernels  227 us (100%)
    pallas_call x1, Pallas kernels, fused(): pl.pallas_call(kernel, out_shape=(vmem((tok_rows, out_w), bf16), vmem((n_...  223 us

profile of v2, /device:TPU:0, one launch (start us, length us, event | category | flops | bytes accessed | tf_op | source)
XLA Modules:
  0.0 227.3 jit_solution(566621269701824592)
XLA Ops:
  0.6 222.6 %fused.1 = (bf16[1024,1536]{1,0:T(8,128)(2,1)S(1)}, bf16[3,3072,384]{2,1,0:T(8,128)(2,1)S(1)}) custom-call(bf16[1024,3072]{1,0:T(8,128)(2,1)} %tok_in.1, f32[1,192]{1,0:T(1,128)} %bitcast.10, f32[8,192,384]{2,1,0:T(8,128)} %w_gate.1, f32[8,192,384]{2,1,0:T(8,128)} %w_up.1, f32[8,192,384]{2,1,0:T(8,128)} %w_down.1, s32[1,1024]{1,0:T(1,128)} %bitcast.9, ...), custom_call_target="tpu_custom_call" | custom-call | tf_op jit(solution)/shard_map/fused/pallas_call | solution.py:384
  223.2 4.0 %deliver.1 = (bf16[1024,1536]{1,0:T(8,128)(2,1)}, bf16[3072,384]{1,0:T(8,128)(2,1)}, bf16[3072,384]{1,0:T(8,128)(2,1)}, bf16[3072,384]{1,0:T(8,128)(2,1)}) custom-call(bf16[1024,1536]{1,0:T(8,128)(2,1)S(1)} %get-tuple-element.10.src, bf16[3,3072,384]{2,1,0:T(8,128)(2,1)S(1)} %get-tuple-element.11.weights), custom_call_target="tpu_custom_call" | custom-call | tf_op jit(solution)/shard_map/deliver/pallas_call | solution.py:451

commit v3 on v2

--- a/solution.py
+++ b/solution.py
@@ -81,7 +81,7 @@
     barrier = pltpu.get_barrier_semaphore()
     for peer in peers:
         pl.semaphore_signal(barrier, inc=1, device_id=peer, device_id_type=pl.DeviceIdType.MESH)
-    pl.semaphore_wait(barrier, len(peers))
+    return lambda: pl.semaphore_wait(barrier, len(peers))
 
 
 def remote(src, dst, send, recv, peer):
@@ -117,11 +117,12 @@
     table = nearest_first(n)
     bf16, f32, i32 = jnp.bfloat16, jnp.float32, jnp.int32
     lanes = 128
+    piece = 512
 
     def kernel(
         tok_in, gain_ref, w_gate, w_up, w_down, gp_ref, ep_ref, rw_ref,
         out, W_own,
-        W_other, wf, ow, tok, outgoing, arrived, aw, pin, ownp, home, h, pcol, wout, wcol,
+        W_other, wf, ow, tok, outgoing, arrived, aw, pin, ownp, home, h, pcol, wout, wcol, mask,
         sends, local, rwz, rwx, rwy, rdx, rdy, rtz, raz, rtt, rat, rp, rh,
     ):
         fs, gr, tp = lax.axis_index("fs"), lax.axis_index("gr"), lax.axis_index("tp")
@@ -147,6 +148,7 @@
             at = pl.multiple_of((x * n_fs + z * members + yy) * rows, rows)
             return W[j].at[:, pl.ds(at, rows), :]
 
+        all_here = greet(z_peers[1:] + [x_peer, y_peer, t_peer])
         w_in = (w_gate, w_up, w_down)
         loads = [
             [
@@ -163,8 +165,6 @@
                 copy.start()
         tok_load = pltpu.make_async_copy(tok_in, tok, local.at[n, 0])
         tok_load.start()
-        greet(z_peers[1:] + [x_peer, y_peer, t_peer])
-
         eye_r = lax.broadcasted_iota(i32, (rows, rows), 0)
         eye_c = lax.broadcasted_iota(i32, (rows, rows), 1)
         gain_col = jnp.sum(jnp.where(eye_r == eye_c, gain_ref[...], 0.0), axis=1, keepdims=True)
@@ -173,7 +173,7 @@
             value = wf[w, s, (y + j) % members]
             return ((gain_col * value) if w < 2 else value).astype(bf16)
 
-        for s in order:
+        def make(s):
             for copy in loads[s]:
                 copy.wait()
             for j in range(members):
@@ -183,6 +183,12 @@
                     else:
                         at = pl.multiple_of((gr * n_fs + fs) * rows, rows)
                         W[j][w, pl.ds(at, rows), :] = cast(s, j, w)
+
+        for s in order:
+            make(s)
+        all_here()
+        for s in order:
+            for j in range(members):
                 if s:
                     send(ow.at[s - 1, j], block(j, gr, y, g), rwz.at[g, j], z_peers[s])
                 else:
@@ -297,7 +303,6 @@
             landed(block(0, gr, other_y, zs[s]), rwy.at[zs[s], 0])
             landed(block(1, other_x, other_y, zs[s]), rdx.at[zs[s]])
             landed(block(0, other_x, other_y, zs[s]), rdy.at[zs[s]])
-        piece = 512
         second = pl.multiple_of(other_t * half, half)
 
         def chunk(s):
@@ -342,31 +347,46 @@
             total = (ownp[...] + pin[s].astype(f32)).astype(bf16)
             if s:
                 back[...] = total
-                send(back, home.at[g], rh.at[g], z_peers[s])
+                for c in range(out_w // piece):
+                    at = pl.ds(c * piece, piece)
+                    send(back.at[:, at], home.at[g, :, at], rh.at[g, c], z_peers[s])
             else:
                 home[g] = total
 
-        def restore(s):
-            z = zs[s]
-
+        def slots_of(z, at):
+            slots = lax.broadcasted_iota(i32, (256, cap), 1) + z * cap
+            return jnp.where(slots == pcol[at, :], 1.0, 0.0).astype(bf16)
+
+        def find(s):
             def rows_of(b, _):
                 at = pl.ds(pl.multiple_of(b * 256, 256), 256)
-                slots = lax.broadcasted_iota(i32, (256, cap), 1) + z * cap
-                back = jnp.where(slots == pcol[at, :], 1.0, 0.0).astype(bf16)
-                value = jnp.dot(back, home[z], preferred_element_type=f32)
+                mask[at, :] = slots_of(zs[s], at)
+                return 0
+
+            lax.fori_loop(0, tok_rows // 256, rows_of, 0)
+
+        def restore(s, c):
+            z = zs[s]
+            cols_at = pl.ds(c * piece, piece)
+
+            def rows_of(b, _):
+                at = pl.ds(pl.multiple_of(b * 256, 256), 256)
+                value = jnp.dot(mask[at, :], home[z, :, cols_at], preferred_element_type=f32)
                 if s:
-                    value += out[at, :].astype(f32)
-                out[at, :] = value.astype(bf16)
+                    value += out[at, cols_at].astype(f32)
+                out[at, cols_at] = value.astype(bf16)
                 return 0
 
             lax.fori_loop(0, tok_rows // 256, rows_of, 0)
 
         for s in [1, 2, 0] + list(range(3, n)):
             chunk(s)
-        for s in range(n):
-            if s:
-                landed(home.at[zs[s]], rh.at[zs[s]])
-            restore(s)
+        for s in [0, 1] + list(range(n - 1, 1, -1)):
+            find(s)
+            for c in range(out_w // piece):
+                if s:
+                    landed(home.at[zs[s], :, pl.ds(c * piece, piece)], rh.at[zs[s], c])
+                restore(s, c)
         for copy in started:
             copy.wait_send()
 
@@ -375,7 +395,7 @@
         + 2 * n
         + (n - 1) * 2 * members + 2 * n
         + 2 * (n - 1)
-        + n + n - 1
+        + n + (n - 1) * (out_w // piece)
     )
     dma = pltpu.SemaphoreType.DMA
     vmem = pltpu.VMEM
@@ -401,6 +421,7 @@
             vmem((tok_rows, 1), i32),
             vmem((n - 1, 8, lanes), f32),
             vmem((members, tok_rows, 1), f32),
+            vmem((tok_rows, cap), bf16),
             dma((n_sends,)),
             dma((n + 1, n_w)),
             dma((n, members)),
@@ -413,7 +434,7 @@
             dma((n,)),
             dma((n,)),
             dma((n,)),
-            dma((n,)),
+            dma((n, out_w // piece)),
         ],
         compiler_params=pltpu.CompilerParams(
             collective_id=0, has_side_effects=True, vmem_limit_bytes=51 * 2**20

time: 228 us -> 227 us (level)
  no operation moved by 1% of the time
where the time goes in v3:
time: 227 us
  Pallas kernels  226 us (100%)
    pallas_call x1, Pallas kernels, fused(): pl.pallas_call(kernel, out_shape=(vmem((tok_rows, out_w), bf16), vmem((n_...  222 us

profile of v3, /device:TPU:0, one launch (start us, length us, event | category | flops | bytes accessed | tf_op | source)
XLA Modules:
  0.0 226.8 jit_solution(6578359974372501390)
XLA Ops:
  0.6 222.0 %fused.1 = (bf16[1024,1536]{1,0:T(8,128)(2,1)S(1)}, bf16[3,3072,384]{2,1,0:T(8,128)(2,1)S(1)}) custom-call(bf16[1024,3072]{1,0:T(8,128)(2,1)} %tok_in.1, f32[1,192]{1,0:T(1,128)} %bitcast.10, f32[8,192,384]{2,1,0:T(8,128)} %w_gate.1, f32[8,192,384]{2,1,0:T(8,128)} %w_up.1, f32[8,192,384]{2,1,0:T(8,128)} %w_down.1, s32[1,1024]{1,0:T(1,128)} %bitcast.9, ...), custom_call_target="tpu_custom_call" | custom-call | tf_op jit(solution)/shard_map/fused/pallas_call | solution.py:404
  222.6 4.0 %deliver.1 = (bf16[1024,1536]{1,0:T(8,128)(2,1)}, bf16[3072,384]{1,0:T(8,128)(2,1)}, bf16[3072,384]{1,0:T(8,128)(2,1)}, bf16[3072,384]{1,0:T(8,128)(2,1)}) custom-call(bf16[1024,1536]{1,0:T(8,128)(2,1)S(1)} %get-tuple-element.10.src, bf16[3,3072,384]{2,1,0:T(8,128)(2,1)S(1)} %get-tuple-element.11.weights), custom_call_target="tpu_custom_call" | custom-call | tf_op jit(solution)/shard_map/deliver/pallas_call | solution.py:472
